TPU v7x, 32 devices: a whole 2x2x4 slice. The times are simulated.
32 devices in a mesh: ep: 8 (over z, y), tp: 4 (over x, core).
Axes of the slice: x: 2, y: 2, z: 4, core: 2. Of those that a mesh axis runs over, the one named last changes fastest.
Arguments:
- tokens: bfloat16 [1024, 2048], P('ep'), may hold values from -6 to 6
- cotangent: bfloat16 [1024, 2048], P('ep'), may hold values from -2 to 2
- route_weights: float32 [1024, 2], P('ep'), may hold values from 0.25 to 2.5
- routes: int32 [1024, 2], P('ep'), may hold values from 0 to 7, all different within a row; in each aligned block of 128 rows (0 to 127, 128 to 255, ...) at most 64 rows name the same one
- gate_proj: bfloat16 [8, 2048, 512], P('ep', None, 'tp'), may hold values from -0.125 to 0.125
- up_proj: bfloat16 [8, 2048, 512], P('ep', None, 'tp'), may hold values from -0.125 to 0.125
- down_proj: bfloat16 [8, 512, 2048], P('ep', 'tp'), may hold values from -0.25 to 0.25
- shared_down: bfloat16 [2048, 512], P(None, 'tp'), may hold values from -0.25 to 0.25
- shared_hidden: bfloat16 [1024, 512], P('ep', 'tp'), may hold values from -0.29882812 to 0.29882812
Outputs:
- tokens_grad: bfloat16 [1024, 2048], P('ep', 'tp')
- weights_grad: float32 [1024, 2], P('ep')
- gate_proj_grad: bfloat16 [8, 2048, 512], P('ep', None, 'tp')
- up_proj_grad: bfloat16 [8, 2048, 512], P('ep', None, 'tp')
- down_proj_grad: bfloat16 [8, 512, 2048], P('ep', 'tp')
- hidden_grad: bfloat16 [1024, 512], P('ep', 'tp')
- shared_grad: float32 [2048, 512], P('ep', 'tp')
Inputs may be any that keep to these rules, and one draw needn't show every extreme that they name: `routes`: in each aligned block of 128 rows no expert is named more than 64 times, a bound that some block reaches; the 2 experts of a row differ.
All inputs are finite; a program needn't handle non-finite values.
Results may differ from a plain program's by a relative error of at most 0.012.
Values may be sent and summed in bfloat16 or wider, within the bound.
A program may use at most 64 MiB of HBM per device.

v0:
```python
import jax
import jax.numpy as jnp
from jax import lax
from jax.sharding import PartitionSpec as P


def shards(
    tokens,
    cotangent,
    route_weights,
    routes,
    gate_proj,
    up_proj,
    down_proj,
    shared_down,
    shared_hidden,
):
    tok_rows, feat_width = tokens.shape
    top_count = routes.shape[1]
    exp_local = gate_proj.shape[0]
    ep_size = lax.axis_size("ep")
    tp_size = lax.axis_size("tp")
    exp_total = exp_local * ep_size
    capacity = 2 * tok_rows * top_count // exp_total
    quarter = feat_width // tp_size
    filled = exp_total * capacity
    flat_routes = routes.reshape(-1)
    one_hot = (flat_routes[:, None] == jnp.arange(exp_total, dtype=jnp.int32)[None, :]).astype(
        jnp.int32
    )
    rank_in = jnp.sum((jnp.cumsum(one_hot, axis=0) - one_hot) * one_hot, axis=1)
    slot_ids = flat_routes * capacity + rank_in
    route_owner = jnp.arange(flat_routes.shape[0], dtype=jnp.int32) // top_count
    owner_ids = jnp.full((filled,), tok_rows, jnp.int32).at[slot_ids].set(route_owner)
    sent_weights = (
        jnp.zeros((filled,), jnp.bfloat16)
        .at[slot_ids]
        .set(route_weights.reshape(-1).astype(jnp.bfloat16))
    )
    first_col = lax.axis_index("tp") * quarter
    own_rows = lax.dynamic_slice_in_dim(tokens, first_col, quarter, 1)
    own_grads = lax.dynamic_slice_in_dim(cotangent, first_col, quarter, 1)
    sent_rows = jnp.take(own_rows, owner_ids, axis=0, mode="fill", fill_value=0)
    sent_grads = jnp.take(own_grads, owner_ids, axis=0, mode="fill", fill_value=0)
    got_rows, got_grads, got_weights = (
        lax.all_to_all(sent_rows, "ep", split_axis=0, concat_axis=0, tiled=True),
        lax.all_to_all(sent_grads, "ep", split_axis=0, concat_axis=0, tiled=True),
        lax.all_to_all(sent_weights, "ep", split_axis=0, concat_axis=0, tiled=True),
    )
    got_rows, got_grads = (
        lax.all_gather(got_rows, "tp", axis=1, tiled=True),
        lax.all_gather(got_grads, "tp", axis=1, tiled=True),
    )
    slot_rows = got_rows.reshape(ep_size, exp_local, capacity, feat_width)
    slot_grads = got_grads.reshape(ep_size, exp_local, capacity, feat_width)
    weight_col = got_weights.reshape(ep_size, exp_local, capacity, 1).astype(jnp.float32)
    gate = jnp.einsum("secd,edf->secf", slot_rows, gate_proj, preferred_element_type=jnp.float32)
    upper = jnp.einsum("secd,edf->secf", slot_rows, up_proj, preferred_element_type=jnp.float32)
    active = jax.nn.silu(gate)
    hidden = (active * upper).astype(jnp.bfloat16)
    backed = jnp.einsum("secd,efd->secf", slot_grads, down_proj, preferred_element_type=jnp.float32)
    gate_share = jnp.sum(hidden.astype(jnp.float32) * backed, axis=3)
    d_hidden = weight_col * backed
    sigma = jax.nn.sigmoid(gate)
    d_gate = (d_hidden * upper * sigma * (1.0 + gate * (1.0 - sigma))).astype(jnp.bfloat16)
    d_up = (d_hidden * active).astype(jnp.bfloat16)
    scaled = (weight_col * slot_grads).astype(jnp.bfloat16)
    down_proj_grad = jnp.einsum(
        "secf,secd->efd", hidden, scaled, preferred_element_type=jnp.float32
    ).astype(jnp.bfloat16)
    gate_proj_grad = jnp.einsum(
        "secd,secf->edf", slot_rows, d_gate, preferred_element_type=jnp.float32
    ).astype(jnp.bfloat16)
    up_proj_grad = jnp.einsum(
        "secd,secf->edf", slot_rows, d_up, preferred_element_type=jnp.float32
    ).astype(jnp.bfloat16)
    partial_value = jnp.einsum(
        "secf,edf->secd", d_gate, gate_proj, preferred_element_type=jnp.float32
    )
    partial_value = partial_value + jnp.einsum(
        "secf,edf->secd", d_up, up_proj, preferred_element_type=jnp.float32
    )
    gate_whole = lax.psum(gate_share, "tp")
    input_cols = lax.psum_scatter(
        partial_value.astype(jnp.bfloat16), "tp", scatter_dimension=3, tiled=True
    )
    back_cols, back_gate = (
        lax.all_to_all(
            input_cols.reshape(filled, quarter), "ep", split_axis=0, concat_axis=0, tiled=True
        ),
        lax.all_to_all(
            gate_whole.astype(jnp.bfloat16).reshape(filled),
            "ep",
            split_axis=0,
            concat_axis=0,
            tiled=True,
        ),
    )
    picked = back_cols[slot_ids].reshape(tok_rows, top_count, quarter)
    tokens_grad = jnp.sum(picked.astype(jnp.float32), axis=1).astype(jnp.bfloat16)
    weights_grad = back_gate[slot_ids].astype(jnp.float32).reshape(tok_rows, top_count)
    hidden_grad = jnp.dot(cotangent, shared_down, preferred_element_type=jnp.float32).astype(
        jnp.bfloat16
    )
    shared_grad = lax.psum_scatter(
        jnp.einsum("td,th->dh", cotangent, shared_hidden, preferred_element_type=jnp.float32),
        "ep",
        scatter_dimension=0,
        tiled=True,
    )
    return (
        tokens_grad,
        weights_grad,
        gate_proj_grad,
        up_proj_grad,
        down_proj_grad,
        hidden_grad,
        shared_grad,
    )


def solution(mesh):
    in_specs = (
        P("ep", None),
        P("ep", None),
        P("ep", None),
        P("ep", None),
        P("ep", None, "tp"),
        P("ep", None, "tp"),
        P("ep", "tp", None),
        P(None, "tp"),
        P("ep", "tp"),
    )
    out_specs = (
        P("ep", "tp"),
        P("ep", None),
        P("ep", None, "tp"),
        P("ep", None, "tp"),
        P("ep", "tp", None),
        P("ep", "tp"),
        P("ep", "tp"),
    )
    return jax.shard_map(shards, mesh=mesh, in_specs=in_specs, out_specs=out_specs, check_vma=False)
```

profile of v0, /device:TPU:0, one launch (start us, length us, event | category | flops | bytes accessed | tf_op | source)
XLA Modules:
  0.0 198.5 jit_solution(4977490238628618403)
XLA Ops:
  7.2 0.0 copy-start
  7.2 0.0 all-gather.5.cloned.1.call-start
  7.2 0.7 broadcast_multiply_fusion
  8.0 0.8 copy.27
  8.8 0.1 eq.29
  8.9 0.1 eq.25
  9.0 0.1 copy.26
  9.2 0.1 mul.68
  9.3 0.6 reduce-window.6
  9.9 0.2 slice_reduce_fusion
  10.1 0.1 fusion.20
  10.3 1.4 scatter_custom_fusion.1
  11.7 0.9 constant_dynamic-slice_fusion
  12.6 0.9 constant_dynamic-slice_fusion.1
  13.6 2.0 gather_fusion.2
  15.5 2.0 gather_fusion.3
  17.5 0.1 broadcast_select_fusion.1
  17.7 0.0 copy-start.8
  17.7 21.7 %all_to_all.58 = bf16[8,64,512]{2,1,0:T(8,128)(2,1)} all-to-all(bf16[8,64,512]{2,1,0:T(8,128)(2,1)S(1)} %bitcast.120), channel_id=1, replica_groups=mesh['ep'=8,'tp'=4] {'ep'}, dimensions={0} | all-to-all | bytes 1048576 | tf_op jit(solution)/shard_map/all_to_all | solution.py:46
  39.4 0.0 all-gather.5.cloned.1.call-update
  39.4 0.0 all-gather.3.cloned.1.call-start
  39.5 0.0 copy-start.3
  39.5 17.8 %all_to_all.59 = bf16[8,64,512]{2,1,0:T(8,128)(2,1)} all-to-all(bf16[8,64,512]{2,1,0:T(8,128)(2,1)S(1)} %bitcast.119), channel_id=1, replica_groups=mesh['ep'=8,'tp'=4] {'ep'}, dimensions={0} | all-to-all | bytes 1048576 | tf_op jit(solution)/shard_map/all_to_all | solution.py:47
  57.3 0.0 all-gather.3.cloned.1.call-update
  57.3 0.0 reduce-scatter.3.cloned.1.call-start
  57.3 0.0 copy-done.8
  57.4 0.1 copy.29
  57.5 0.1 reshape.210
  57.6 2.2 %scatter_custom_fusion = bf16[512]{0:T(512)(128)(2,1)S(1)} fusion(s32[256]{0:T(256)S(1)} %bitcast.130, bf16[256]{0:T(256)(128)(2,1)S(1)} %reshape.210, bf16[]{:T(256)} %constant.23.clone.1), kind=kCustom, calls=%fused_computation.63 | custom fusion | bytes 1026 | tf_op jit(solution)/shard_map/scatter | solution.py:38
  59.8 0.1 all_to_all.52
  59.9 9.9 %all_to_all.60 = bf16[8,64,1]{1,2,0:T(2,128)(2,1)S(1)} all-to-all(bf16[8,64,1]{1,2,0:T(2,128)(2,1)S(1)} %all_to_all.52), channel_id=1, replica_groups=mesh['ep'=8,'tp'=4] {'ep'}, dimensions={0} | all-to-all | bytes 2048 | tf_op jit(solution)/shard_map/all_to_all | solution.py:48
  69.8 0.0 copy-done
  69.8 2.8 %convolution_bitcast_fusion.3 = f32[8,1,64,128]{3,2,0,1:T(8,128)S(1)} fusion(bf16[8,64,2048]{2,1,0:T(8,128)(2,1)} %bitcast.115, bf16[1,2048,128]{2,1,0:T(8,128)(2,1)S(1)} %copy-done), kind=kOutput, calls=%fused_computation.19 | convolution fusion | flops 268435456 | bytes 2883584 | tf_op jit(solution)/shard_map/secd,edf->secf/dot_general | solution.py:57
  72.6 0.0 copy-done.3
  72.6 1.4 convolution_bitcast_fusion.4
  74.0 11.3 %all-gather.3.cloned.1.call-done = bf16[512,2048]{1,0:T(8,128)(2,1)} async-done(((bf16[512,512]{1,0:T(8,128)(2,1)}), bf16[512,2048]{1,0:T(8,128)(2,1)}) %all-gather.3.cloned.1.call-update) | async-done | bytes 2097168 | tf_op jit(solution)/shard_map/all_gather | solution.py:52
  85.3 3.1 %multiply_reduce_fusion = (f32[8,64]{1,0:T(8,128)S(1)}, bf16[8,1,64,128]{3,2,0,1:T(8,128)(2,1)}, bf16[8,1,64,128]{3,2,0,1:T(8,128)(2,1)S(1)}, bf16[8,64,128]{2,1,0:T(8,128)(2,1)S(1)}) fusion(f32[8,1,64,128]{3,2,0,1:T(8,128)} %convolution_bitcast_fusion.4, f32[8,1,64,128]{3,2,0,1:T(8,128)S(1)} %convolution_bitcast_fusion.3, f32[8,64]{1,0:T(8,128)S(1)} %bitcast.126, ...), kind=kOutput, calls=%fused_computation.31 | convolution fusion | flops 269680128 | bytes 3543040 | tf_op jit(solution)/shard_map/secd,efd->secf/dot_general | solution.py:61
  88.5 0.7 fusion.8
  89.2 0.0 copy-done.4
  89.2 2.0 %fusion = bf16[8,1,64,2048]{3,2,0,1:T(8,128)(2,1)} fusion(f32[8,64,2048]{2,1,0:T(8,128)S(1)} %fusion.8, bf16[8,64,128]{2,1,0:T(8,128)(2,1)S(1)} %get-tuple-element.32, bf16[1,2048,128]{2,1,0:T(8,128)(2,1)S(1)} %copy-done.3), kind=kOutput, calls=%fused_computation.8 | convolution fusion | flops 270532608 | bytes 6946816 | tf_op jit(solution)/shard_map/secf,edf->secd/dot_general | solution.py:80
  91.2 0.0 reduce-scatter.3.cloned.1.call-update
  91.2 0.0 copy-start.6
  91.2 0.0 reduce-scatter.5.cloned.1.call-start
  91.3 1.0 copy-done.2
  92.2 1.3 fusion.28
  93.6 0.0 reduce-scatter.5.cloned.1.call-update
  93.6 5.9 %psum.7 = bf16[8,1,64]{2,0,1:T(8,128)(2,1)S(1)} all-reduce(f32[8,1,64]{2,0,1:T(8,128)S(1)} %bitcast.132), channel_id=1, replica_groups=mesh['ep'=8,'tp'=4] {'tp'}, use_global_device_ids=true, to_apply=%region_8.10 | all-reduce | flops 512 | bytes 3072 | tf_op jit(solution)/shard_map/psum | solution.py:83
  99.5 12.0 %all_to_all.61 = bf16[8,64,1]{1,2,0:T(2,128)(2,1)S(1)} all-to-all(bf16[8,64,1]{1,2,0:T(2,128)(2,1)S(1)} %copy.31), channel_id=1, replica_groups=mesh['ep'=8,'tp'=4] {'ep'}, dimensions={0} | all-to-all | bytes 2048 | tf_op jit(solution)/shard_map/all_to_all | solution.py:91
  111.4 11.1 %reduce-scatter.3.cloned.1.call-done = bf16[8,1,64,512]{3,2,0,1:T(8,128)(2,1)} async-done(((bf16[8,1,64,2048]{3,2,0,1:T(8,128)(2,1)}), bf16[8,1,64,512]{3,2,0,1:T(8,128)(2,1)}) %reduce-scatter.3.cloned.1.call-update) | async-done | bytes 524304 | tf_op jit(solution)/shard_map/reduce_scatter | solution.py:84
  122.6 5.5 %all-to-all-start.3 = ((bf16[8,64,512]{2,1,0:T(8,128)(2,1)}), bf16[8,64,512]{2,1,0:T(8,128)(2,1)S(1)}, u32[]{:S(2)}, u32[]{:S(2)}) async-start(bf16[8,64,512]{2,1,0:T(8,128)(2,1)} %bitcast.125), calls=%async_computation.4 | async-start | bytes 1048576 | tf_op jit(solution)/shard_map/all_to_all | solution.py:88
  128.1 2.1 %convolution_convert_fusion = bf16[128,128]{1,0:T(8,128)(2,1)} fusion(bf16[128,2048]{1,0:T(8,128)(2,1)} %param.12, bf16[2048,128]{1,0:T(8,128)(2,1)} %param.18), kind=kOutput, calls=%fused_computation.22 | convolution fusion | flops 67125248 | bytes 1081344 | tf_op jit(solution)/shard_map/dot_general | solution.py:102
  130.2 0.0 copy-done.6
  130.2 3.0 %fusion.4 = bf16[1,128,2048]{2,1,0:T(8,128)(2,1)} fusion(bf16[8,64,2048]{2,1,0:T(8,128)(2,1)} %bitcast.122, f32[8,64]{1,0:T(8,128)S(1)} %bitcast.127, bf16[8,1,64,128]{3,2,0,1:T(8,128)(2,1)S(1)} %copy-done.6), kind=kOutput, calls=%fused_computation.15 | convolution fusion | flops 271843328 | bytes 2754560 | tf_op jit(solution)/shard_map/secf,secd->efd/dot_general | solution.py:68
  133.2 1.6 fusion.6
  134.8 1.6 fusion.5
  136.4 0.1 all_to_all.51
  136.5 1.9 gather_fusion.1
  138.4 0.1 reshape.173
  138.5 0.6 copy.32
  139.2 7.2 %all-to-all-done.3 = bf16[8,64,512]{2,1,0:T(8,128)(2,1)S(1)} async-done(((bf16[8,64,512]{2,1,0:T(8,128)(2,1)}), bf16[8,64,512]{2,1,0:T(8,128)(2,1)S(1)}, u32[]{:S(2)}, u32[]{:S(2)}) %all-to-all-start.3) | async-done | bytes 524320 | tf_op jit(solution)/shard_map/all_to_all | solution.py:88
  146.4 1.2 gather_fusion
  147.5 0.1 reshape.170
  147.6 1.3 reduce_sum.36
  148.9 43.0 %reduce-scatter.5.cloned.1.call-done = f32[256,128]{1,0:T(8,128)} async-done(((f32[2048,128]{1,0:T(8,128)}), f32[256,128]{1,0:T(8,128)}) %reduce-scatter.5.cloned.1.call-update) | async-done | bytes 131088 | tf_op jit(solution)/shard_map/reduce_scatter | solution.py:105
  (22 shorter events, 0.1 us)
Async XLA Ops:
  7.2 62.7 %copy-start = (bf16[1,2048,128]{2,1,0:T(8,128)(2,1)S(1)}, bf16[1,2048,128]{2,1,0:T(8,128)(2,1)}, u32[]{:S(2)}) copy-start(bf16[1,2048,128]{2,1,0:T(8,128)(2,1)} %param.15) | copy-start | bytes 1572868
  7.2 62.6 %all-gather.5.cloned.1.call-start = ((), (), s32[]{:S(2)}) async-start(), calls=%async_computation.8 | async-start | bytes 2621440 | tf_op jit(solution)/shard_map/all_gather | solution.py:51
  17.7 39.7 %copy-start.8 = (f32[128,2]{0,1:T(2,128)S(1)}, f32[128,2]{0,1:T(2,128)}, u32[]{:S(2)}) copy-start(f32[128,2]{0,1:T(2,128)} %param.13) | copy-start | bytes 3076
  39.4 45.9 %all-gather.3.cloned.1.call-start = ((), (), s32[]{:S(2)}) async-start(), calls=%async_computation.7 | async-start | bytes 2621440 | tf_op jit(solution)/shard_map/all_gather | solution.py:52
  39.5 33.1 %copy-start.3 = (bf16[1,2048,128]{2,1,0:T(8,128)(2,1)S(1)}, bf16[1,2048,128]{2,1,0:T(8,128)(2,1)}, u32[]{:S(2)}) copy-start(bf16[1,2048,128]{2,1,0:T(8,128)(2,1)} %param.16) | copy-start | bytes 1572868
  57.3 65.3 %reduce-scatter.3.cloned.1.call-start = ((), (), s32[]{:S(2)}) async-start(), calls=%async_computation.9 | async-start | bytes 2621440 | tf_op jit(solution)/shard_map/reduce_scatter | solution.py:84
  69.8 2.8 %copy-start.1 = (bf16[512,2048]{1,0:T(8,128)(2,1)S(1)}, bf16[512,2048]{1,0:T(8,128)(2,1)}, u32[]{:S(2)}) copy-start(bf16[512,2048]{1,0:T(8,128)(2,1)} %all-gather.5.cloned.1.call-done) | copy-start | bytes 6291460
  88.5 0.7 copy-start.4
  91.2 1.0 copy-start.2
  91.2 1.0 copy-start.7
  91.2 39.0 %copy-start.6 = (bf16[8,1,64,128]{3,2,0,1:T(8,128)(2,1)S(1)}, bf16[8,1,64,128]{3,2,0,1:T(8,128)(2,1)}, u32[]{:S(2)}) copy-start(bf16[8,1,64,128]{3,2,0,1:T(8,128)(2,1)} %get-tuple-element.30) | copy-start | bytes 393220
  91.2 100.7 %reduce-scatter.5.cloned.1.call-start = ((), (), s32[]{:S(2)}) async-start(), calls=%async_computation.10 | async-start | bytes 1179648 | tf_op jit(solution)/shard_map/reduce_scatter | solution.py:105
  122.6 23.8 %all-to-all-start.3 = ((bf16[8,64,512]{2,1,0:T(8,128)(2,1)}), bf16[8,64,512]{2,1,0:T(8,128)(2,1)S(1)}, u32[]{:S(2)}, u32[]{:S(2)}) async-start(bf16[8,64,512]{2,1,0:T(8,128)(2,1)} %bitcast.125), calls=%async_computation.4 | async-start | bytes 1048576 | tf_op jit(solution)/shard_map/all_to_all | solution.py:88
  128.1 5.2 %copy-start.5 = (bf16[8,1,64,128]{3,2,0,1:T(8,128)(2,1)S(1)}, bf16[8,1,64,128]{3,2,0,1:T(8,128)(2,1)}, u32[]{:S(2)}) copy-start(bf16[8,1,64,128]{3,2,0,1:T(8,128)(2,1)} %copy-done.4) | copy-start | bytes 393220
Sparse Core Ops, SparseCore 0:
  39.6 21.5 all-gather.4
  62.7 22.5 all-gather.2
  91.3 31.1 reduce-scatter.2
  126.4 65.4 reduce-scatter.4
where the time goes:
time: 199 us; the launch traced here: 198 us
  waiting for transfers between devices  72.6 us (36%)
  blocking collectives  67.3 us (34%)
  matrix products  19.6 us (10%)
  local copies, waits for them, and re-layouts  16.3 us (8%)
  between operations  14 us (7%)
  starting transfers between devices  5.68 us (3%)
  other arithmetic  2.98 us (1%)
    reduce_scatter x1, waiting for transfers between devices, shards(): lax.psum_scatter(jnp.einsum('td,th->dh', cotangent, shared_hidden, prefer...  43 us
    all_to_all x1, blocking collectives, shards(): lax.all_to_all(sent_rows, 'ep', split_axis=0, concat_axis=0, tiled=True)  21.7 us
    all_to_all x1, blocking collectives, shards(): lax.all_to_all(sent_grads, 'ep', split_axis=0, concat_axis=0, tiled=True)  17.8 us
    all_to_all x1, blocking collectives, shards(): lax.all_to_all(gate_whole.astype(jnp.bfloat16).reshape(filled), 'ep', spl...  12 us
    all_gather x1, waiting for transfers between devices, shards(): lax.all_gather(got_grads, 'tp', axis=1, tiled=True)  11.3 us
    reduce_scatter x1, waiting for transfers between devices, shards(): lax.psum_scatter(partial_value.astype(jnp.bfloat16), 'tp', scatter_dimens...  11.1 us
    all_to_all x1, blocking collectives, shards(): lax.all_to_all(sent_weights, 'ep', split_axis=0, concat_axis=0, tiled=True)  9.92 us
    all_to_all x1, waiting for transfers between devices, shards(): lax.all_to_all(input_cols.reshape(filled, quarter), 'ep', split_axis=0, c...  7.17 us
  transfers between devices with their start and end apart: 5, of which 4 were waited for; matrix products, arithmetic and copies ran while one was open for 11% of the time, Pallas kernels for 0%

commit v1 on v0

--- a/solution.py
+++ b/solution.py
@@ -49,7 +49,7 @@
     )
     got_rows, got_grads = (
         lax.all_gather(got_rows, "tp", axis=1, tiled=True),
-        lax.all_gather(got_grads, "tp", axis=1, tiled=True),
+        jnp.concatenate(lax.all_gather(got_grads, "tp"), axis=1),
     )
     slot_rows = got_rows.reshape(ep_size, exp_local, capacity, feat_width)
     slot_grads = got_grads.reshape(ep_size, exp_local, capacity, feat_width)

time: 199 us -> 201 us (1.010)
  local copies, waits for them, and re-layouts: 16.3 us -> 23.6 us
  matrix products: 19.6 us -> 17 us
  waiting for transfers between devices: 72.6 us -> 70 us
    all_gather x1, waiting for transfers between devices: 11.3 us -> 0.01 us  [shards(): lax.all_gather(got_grads, 'tp')]
    all_gather x1, waiting for transfers between devices: 0.01 us -> 9.29 us  [shards(): lax.all_gather(got_rows, 'tp', axis=1, tiled=True)]
    all_to_all x1, blocking collectives: 21.7 us -> 17.6 us  [shards(): lax.all_to_all(sent_rows, 'ep', split_axis=0, concat_axis=0, tiled=True)]
    all_to_all x1, blocking collectives: 17.8 us -> 21.7 us  [shards(): lax.all_to_all(sent_grads, 'ep', split_axis=0, concat_axis=0, tiled=True)]
    reshape x0 -> x1, local copies, waits for them, and re-layouts: none -> 3.54 us  [shards(): jnp.concatenate(lax.all_gather(got_grads, 'tp'), axis=1)]
    another operation x1 -> x2, local copies, waits for them, and re-layouts: 0.01 us -> 2.81 us
    dot_general x1, matrix products: 3.13 us -> 0.8 us  [shards(): jnp.einsum('secd,efd->secf', slot_grads, down_proj, preferred_element_typ...]
  transfers between devices with their start and end apart: 5 -> 5, of which waited for: 4 -> 4; matrix products, arithmetic and copies ran while one was open for 11% -> 12% of each run, Pallas kernels for 0% -> 0%
where the time goes in v1:
time: 201 us; the launch traced here: 200 us
  waiting for transfers between devices  70 us (35%)
  blocking collectives  67.1 us (33%)
  local copies, waits for them, and re-layouts  23.6 us (12%)
  matrix products  17 us (8%)
  between operations  14 us (7%)
  starting transfers between devices  5.68 us (3%)
  other arithmetic  2.98 us (1%)
    reduce_scatter x1, waiting for transfers between devices, shards(): lax.psum_scatter(jnp.einsum('td,th->dh', cotangent, shared_hidden, prefer...  42.9 us
    all_to_all x1, blocking collectives, shards(): lax.all_to_all(sent_grads, 'ep', split_axis=0, concat_axis=0, tiled=True)  21.7 us
    all_to_all x1, blocking collectives, shards(): lax.all_to_all(sent_rows, 'ep', split_axis=0, concat_axis=0, tiled=True)  17.6 us
    all_to_all x1, blocking collectives, shards(): lax.all_to_all(gate_whole.astype(jnp.bfloat16).reshape(filled), 'ep', spl...  12 us
    reduce_scatter x1, waiting for transfers between devices, shards(): lax.psum_scatter(partial_value.astype(jnp.bfloat16), 'tp', scatter_dimens...  10.4 us
    all_to_all x1, blocking collectives, shards(): lax.all_to_all(sent_weights, 'ep', split_axis=0, concat_axis=0, tiled=True)  9.92 us
    all_gather x1, waiting for transfers between devices, shards(): lax.all_gather(got_rows, 'tp', axis=1, tiled=True)  9.29 us
    all_to_all x1, waiting for transfers between devices, shards(): lax.all_to_all(input_cols.reshape(filled, quarter), 'ep', split_axis=0, c...  7.31 us
  transfers between devices with their start and end apart: 5, of which 4 were waited for; matrix products, arithmetic and copies ran while one was open for 12% of the time, Pallas kernels for 0%

profile of v1, /device:TPU:0, one launch (start us, length us, event | category | flops | bytes accessed | tf_op | source)
XLA Modules:
  0.0 200.3 jit_solution(3969692730079740952)
XLA Ops:
  7.2 0.0 copy-start
  7.2 0.0 all-gather.3.cloned.1.call-start
  7.2 0.7 broadcast_multiply_fusion
  8.0 0.8 copy.29
  8.8 0.1 eq.29
  8.9 0.1 eq.25
  9.0 0.1 copy.28
  9.2 0.1 mul.68
  9.3 0.6 reduce-window.6
  9.9 0.2 slice_reduce_fusion
  10.1 0.1 fusion.20
  10.3 1.4 scatter_custom_fusion.1
  11.7 0.9 constant_dynamic-slice_fusion
  12.6 0.9 constant_dynamic-slice_fusion.1
  13.6 2.0 gather_fusion.2
  15.5 2.0 gather_fusion.3
  17.5 0.1 broadcast_select_fusion.1
  17.7 0.0 copy-start.6
  17.7 21.7 %all_to_all.55 = bf16[8,64,512]{2,1,0:T(8,128)(2,1)} all-to-all(bf16[8,64,512]{2,1,0:T(8,128)(2,1)S(1)} %bitcast.120), channel_id=1, replica_groups=mesh['ep'=8,'tp'=4] {'ep'}, dimensions={0} | all-to-all | bytes 1048576 | tf_op jit(solution)/shard_map/all_to_all | solution.py:47
  39.4 0.0 all-gather.3.cloned.1.call-update
  39.4 0.0 all-gather.5.cloned.1.call-start
  39.5 17.6 %all_to_all.56 = bf16[8,64,512]{2,1,0:T(8,128)(2,1)} all-to-all(bf16[8,64,512]{2,1,0:T(8,128)(2,1)S(1)} %bitcast.119), channel_id=1, replica_groups=mesh['ep'=8,'tp'=4] {'ep'}, dimensions={0} | all-to-all | bytes 1048576 | tf_op jit(solution)/shard_map/all_to_all | solution.py:46
  57.1 0.0 all-gather.5.cloned.1.call-update
  57.1 0.0 reduce-scatter.3.cloned.1.call-start
  57.2 0.0 copy-done.6
  57.2 0.1 copy.31
  57.4 0.1 reshape.214
  57.5 2.2 %scatter_custom_fusion = bf16[512]{0:T(512)(128)(2,1)S(1)} fusion(s32[256]{0:T(256)S(1)} %bitcast.129, bf16[256]{0:T(256)(128)(2,1)S(1)} %reshape.214, bf16[]{:T(256)} %constant.23.clone.1), kind=kCustom, calls=%fused_computation.63 | custom fusion | bytes 1026 | tf_op jit(solution)/shard_map/scatter | solution.py:38
  59.7 0.1 all_to_all.49
  59.8 9.9 %all_to_all.57 = bf16[8,64,1]{1,2,0:T(2,128)(2,1)S(1)} all-to-all(bf16[8,64,1]{1,2,0:T(2,128)(2,1)S(1)} %all_to_all.49), channel_id=1, replica_groups=mesh['ep'=8,'tp'=4] {'ep'}, dimensions={0} | all-to-all | bytes 2048 | tf_op jit(solution)/shard_map/all_to_all | solution.py:48
  69.7 3.5 %copy.33 = bf16[512,4,512]{2,1,0:T(4,128)(2,1)S(1)} copy(bf16[512,4,512]{2,0,1:T(8,128)(2,1)} %bitcast.121) | data formatting | bytes 4194304 | tf_op jit(solution)/shard_map/reshape | solution.py:52
  73.2 2.8 %reshape.167 = bf16[8,64,2048]{2,1,0:T(8,128)(2,1)} reshape(bf16[512,4,512]{2,1,0:T(4,128)(2,1)S(1)} %copy.33) | data formatting | bytes 4194304 | tf_op jit(solution)/shard_map/reshape.6
  76.0 9.3 %all-gather.5.cloned.1.call-done = bf16[512,2048]{1,0:T(8,128)(2,1)} async-done(((bf16[512,512]{1,0:T(8,128)(2,1)}), bf16[512,2048]{1,0:T(8,128)(2,1)}) %all-gather.5.cloned.1.call-update) | async-done | bytes 2097168 | tf_op jit(solution)/shard_map/all_gather | solution.py:51
  85.3 0.0 copy-done
  85.3 2.4 %convolution_bitcast_fusion.3 = f32[8,1,64,128]{3,2,0,1:T(8,128)S(1)} fusion(bf16[8,64,2048]{2,1,0:T(8,128)(2,1)} %bitcast.115, bf16[1,2048,128]{2,1,0:T(8,128)(2,1)S(1)} %copy-done), kind=kOutput, calls=%fused_computation.19 | convolution fusion | flops 268435456 | bytes 2883584 | tf_op jit(solution)/shard_map/secd,edf->secf/dot_general | solution.py:57
  87.8 0.0 copy-start.5
  87.8 0.7 convolution_bitcast_fusion.4
  88.5 0.9 copy-done.2
  89.4 0.1 copy-done.5
  89.5 0.8 multiply_reduce_fusion
  90.3 0.7 fusion.8
  91.0 2.0 %fusion = bf16[8,1,64,2048]{3,2,0,1:T(8,128)(2,1)} fusion(f32[8,64,2048]{2,1,0:T(8,128)S(1)} %fusion.8, bf16[8,64,128]{2,1,0:T(8,128)(2,1)S(1)} %get-tuple-element.32, bf16[1,2048,128]{2,1,0:T(8,128)(2,1)S(1)} %copy-done.4), kind=kOutput, calls=%fused_computation.8 | convolution fusion | flops 270532608 | bytes 6946816 | tf_op jit(solution)/shard_map/secf,edf->secd/dot_general | solution.py:80
  93.0 0.0 reduce-scatter.3.cloned.1.call-update
  93.0 0.0 reduce-scatter.5.cloned.1.call-start
  93.1 1.0 copy-done.3
  94.0 2.1 %fusion.28 = f32[2048,128]{1,0:T(8,128)} fusion(bf16[128,2048]{1,0:T(8,128)(2,1)S(1)} %copy-done.3, bf16[128,128]{1,0:T(8,128)(2,1)} %param.19), kind=kOutput, calls=%fused_computation.65 | convolution fusion | flops 67108864 | bytes 1605632 | tf_op jit(solution)/shard_map/td,th->dh/dot_general | solution.py:106
  96.1 0.0 reduce-scatter.5.cloned.1.call-update
  96.1 5.9 %psum.7 = bf16[8,1,64]{2,0,1:T(8,128)(2,1)S(1)} all-reduce(f32[8,1,64]{2,0,1:T(8,128)S(1)} %bitcast.131), channel_id=1, replica_groups=mesh['ep'=8,'tp'=4] {'tp'}, use_global_device_ids=true, to_apply=%region_8.10 | all-reduce | flops 512 | bytes 3072 | tf_op jit(solution)/shard_map/psum | solution.py:83
  102.0 12.0 %all_to_all.58 = bf16[8,64,1]{1,2,0:T(2,128)(2,1)S(1)} all-to-all(bf16[8,64,1]{1,2,0:T(2,128)(2,1)S(1)} %copy.34), channel_id=1, replica_groups=mesh['ep'=8,'tp'=4] {'ep'}, dimensions={0} | all-to-all | bytes 2048 | tf_op jit(solution)/shard_map/all_to_all | solution.py:91
  114.0 10.4 %reduce-scatter.3.cloned.1.call-done = bf16[8,1,64,512]{3,2,0,1:T(8,128)(2,1)} async-done(((bf16[8,1,64,2048]{3,2,0,1:T(8,128)(2,1)}), bf16[8,1,64,512]{3,2,0,1:T(8,128)(2,1)}) %reduce-scatter.3.cloned.1.call-update) | async-done | bytes 524304 | tf_op jit(solution)/shard_map/reduce_scatter | solution.py:84
  124.4 5.5 %all-to-all-start.3 = ((bf16[8,64,512]{2,1,0:T(8,128)(2,1)}), bf16[8,64,512]{2,1,0:T(8,128)(2,1)S(1)}, u32[]{:S(2)}, u32[]{:S(2)}) async-start(bf16[8,64,512]{2,1,0:T(8,128)(2,1)} %bitcast.124), calls=%async_computation.4 | async-start | bytes 1048576 | tf_op jit(solution)/shard_map/all_to_all | solution.py:88
  129.9 2.1 %convolution_convert_fusion = bf16[128,128]{1,0:T(8,128)(2,1)} fusion(bf16[128,2048]{1,0:T(8,128)(2,1)} %param.12, bf16[2048,128]{1,0:T(8,128)(2,1)} %param.18), kind=kOutput, calls=%fused_computation.22 | convolution fusion | flops 67125248 | bytes 1081344 | tf_op jit(solution)/shard_map/dot_general | solution.py:102
  132.0 3.0 %fusion.4 = bf16[1,128,2048]{2,1,0:T(8,128)(2,1)} fusion(bf16[8,64,2048]{2,1,0:T(8,128)(2,1)} %reshape.167, f32[8,64]{1,0:T(8,128)S(1)} %bitcast.126, bf16[8,1,64,128]{3,2,0,1:T(8,128)(2,1)S(1)} %get-tuple-element.30), kind=kOutput, calls=%fused_computation.15 | convolution fusion | flops 271843328 | bytes 2754560 | tf_op jit(solution)/shard_map/secf,secd->efd/dot_general | solution.py:68
  135.0 1.6 fusion.6
  136.5 1.6 fusion.5
  138.1 0.1 all_to_all.48
  138.2 1.9 gather_fusion.1
  140.1 0.1 reshape.177
  140.3 0.6 copy.35
  140.9 7.3 %all-to-all-done.3 = bf16[8,64,512]{2,1,0:T(8,128)(2,1)S(1)} async-done(((bf16[8,64,512]{2,1,0:T(8,128)(2,1)}), bf16[8,64,512]{2,1,0:T(8,128)(2,1)S(1)}, u32[]{:S(2)}, u32[]{:S(2)}) %all-to-all-start.3) | async-done | bytes 524320 | tf_op jit(solution)/shard_map/all_to_all | solution.py:88
  148.2 1.2 gather_fusion
  149.4 0.1 reshape.174
  149.5 1.3 reduce_sum.36
  150.8 42.9 %reduce-scatter.5.cloned.1.call-done = f32[256,128]{1,0:T(8,128)} async-done(((f32[2048,128]{1,0:T(8,128)}), f32[256,128]{1,0:T(8,128)}) %reduce-scatter.5.cloned.1.call-update) | async-done | bytes 131088 | tf_op jit(solution)/shard_map/reduce_scatter | solution.py:105
  (20 shorter events, 0.1 us)
Async XLA Ops:
  7.2 78.2 %copy-start = (bf16[1,2048,128]{2,1,0:T(8,128)(2,1)S(1)}, bf16[1,2048,128]{2,1,0:T(8,128)(2,1)}, u32[]{:S(2)}) copy-start(bf16[1,2048,128]{2,1,0:T(8,128)(2,1)} %param.15) | copy-start | bytes 1572868
  7.2 62.5 %all-gather.3.cloned.1.call-start = ((), (), s32[]{:S(2)}) async-start(), calls=%async_computation.7 | async-start | bytes 2621440 | tf_op jit(solution)/shard_map/all_gather | solution.py:52
  17.7 39.5 %copy-start.6 = (f32[128,2]{0,1:T(2,128)S(1)}, f32[128,2]{0,1:T(2,128)}, u32[]{:S(2)}) copy-start(f32[128,2]{0,1:T(2,128)} %param.13) | copy-start | bytes 3076
  39.4 45.9 %all-gather.5.cloned.1.call-start = ((), (), s32[]{:S(2)}) async-start(), calls=%async_computation.8 | async-start | bytes 2621440 | tf_op jit(solution)/shard_map/all_gather | solution.py:51
  57.1 67.2 %reduce-scatter.3.cloned.1.call-start = ((), (), s32[]{:S(2)}) async-start(), calls=%async_computation.9 | async-start | bytes 2621440 | tf_op jit(solution)/shard_map/reduce_scatter | solution.py:84
  76.0 11.7 %copy-start.4 = (bf16[1,2048,128]{2,1,0:T(8,128)(2,1)S(1)}, bf16[1,2048,128]{2,1,0:T(8,128)(2,1)}, u32[]{:S(2)}) copy-start(bf16[1,2048,128]{2,1,0:T(8,128)(2,1)} %param.16) | copy-start | bytes 1572868
  85.3 2.5 %copy-start.1 = (bf16[512,2048]{1,0:T(8,128)(2,1)S(1)}, bf16[512,2048]{1,0:T(8,128)(2,1)}, u32[]{:S(2)}) copy-start(bf16[512,2048]{1,0:T(8,128)(2,1)} %all-gather.5.cloned.1.call-done) | copy-start | bytes 6291460
  87.8 1.6 copy-start.2
  87.8 1.7 copy-start.5
  93.0 1.0 copy-start.3
  93.0 100.7 %reduce-scatter.5.cloned.1.call-start = ((), (), s32[]{:S(2)}) async-start(), calls=%async_computation.10 | async-start | bytes 1179648 | tf_op jit(solution)/shard_map/reduce_scatter | solution.py:105
  124.4 23.9 %all-to-all-start.3 = ((bf16[8,64,512]{2,1,0:T(8,128)(2,1)}), bf16[8,64,512]{2,1,0:T(8,128)(2,1)S(1)}, u32[]{:S(2)}, u32[]{:S(2)}) async-start(bf16[8,64,512]{2,1,0:T(8,128)(2,1)} %bitcast.124), calls=%async_computation.4 | async-start | bytes 1048576 | tf_op jit(solution)/shard_map/all_to_all | solution.py:88
Sparse Core Ops, SparseCore 0:
  39.6 21.5 all-gather.2
  62.7 22.5 all-gather.4
  93.2 31.1 reduce-scatter.2
  128.2 65.5 reduce-scatter.4
